TPU v7x, 256 devices: a 2x2x32 block of a 4x8x32 slice. The times are simulated.
256 devices in a mesh: grp: 4 (over y, x), ep: 32 (over z), tp: 2 (over core).
Axes of the slice: x: 2, y: 2, z: 32, core: 2. Of those that a mesh axis runs over, the one named last changes fastest.
The devices are a block of a 4x8x32 slice.
Arguments:
- tokens: bfloat16 [65536, 2048], P(('grp', 'ep', 'tp')), parts along dimension 0, may hold values from -6 to 6
- norm_gain: float32 [2048], replicated, may hold values from 0.1 to 1.9
- expert_ids: int32 [65536, 4], P(('grp', 'ep', 'tp')), parts along dimension 0, may hold values from 0 to 31, all different within a row; in each aligned block of 256 rows (0 to 255, 256 to 511, ...) at most 40 rows name the same one
- gate_weights: float32 [65536, 4], P(('grp', 'ep', 'tp')), parts along dimension 0, may hold values from 0.1 to 1
- expert_gate: bfloat16 [32, 2048, 512], P('ep', None, 'tp'), may hold values from -0.125 to 0.125
- expert_up: bfloat16 [32, 2048, 512], P('ep', None, 'tp'), may hold values from -0.125 to 0.125
- expert_down: bfloat16 [32, 512, 2048], P('ep', 'tp'), may hold values from -0.25 to 0.25
- shared_gate: bfloat16 [2048, 512], replicated, may hold values from -0.125 to 0.125
- shared_up: bfloat16 [2048, 512], replicated, may hold values from -0.125 to 0.125
- shared_down: bfloat16 [512, 2048], replicated, may hold values from -0.25 to 0.25
- post_gain: float32 [2048], replicated, may hold values from 0.1 to 1.9
Outputs:
- mixed: bfloat16 [65536, 2048], P(('grp', 'ep', 'tp')), parts along dimension 0
There are 4 independent parts, one for each index of `grp`. A program takes and returns all parts, laid end to end along the dimension named above; an argument that names none is the same for every part. Nothing has to cross between parts.
Inputs may be any that keep to these rules, and one draw needn't show every extreme that they name: `expert_ids`: each row names 4 different experts; in each device's aligned block of 256 rows no expert is named by more than 40 rows, a bound that some block reaches.
All inputs are finite; a program needn't handle non-finite values.
Results may differ from a plain program's by a relative error of at most 0.0067.
Values may be sent and summed in bfloat16 or wider, within the bound.
A program may use at most 128 MiB of HBM per device.

v0:
```python
import jax
import jax.numpy as jnp
from jax import lax
from jax.sharding import PartitionSpec as P

EXPERTS = 32
CAP = 40


EPS = 1e-06


def rms_scale(inputs, gain):
    mean_sq = jnp.mean(inputs * inputs, axis=-1, keepdims=True)
    return inputs * lax.rsqrt(mean_sq + EPS) * gain


def expert_rows(tok_rows, w_gate, w_up, w_down):
    gate_act = jnp.einsum("erd,edf->erf", tok_rows, w_gate, preferred_element_type=jnp.float32)
    up_act = jnp.einsum("erd,edf->erf", tok_rows, w_up, preferred_element_type=jnp.float32)
    hidden = (jax.nn.silu(gate_act) * up_act).astype(jnp.bfloat16)
    return jnp.einsum("erf,efd->erd", hidden, w_down, preferred_element_type=jnp.float32)


def shared_branch(normed, shared_gate, shared_up, shared_down):
    shared_act = jnp.dot(normed, shared_gate, preferred_element_type=jnp.float32)
    shared_lift = jnp.dot(normed, shared_up, preferred_element_type=jnp.float32)
    shared_hidden = (jax.nn.silu(shared_act) * shared_lift).astype(jnp.bfloat16)
    return jnp.dot(shared_hidden, shared_down, preferred_element_type=jnp.float32)


def body(
    tokens,
    norm_gain,
    expert_ids,
    gate_weights,
    expert_gate,
    expert_up,
    expert_down,
    shared_gate,
    shared_up,
    shared_down,
    post_gain,
):
    tok_count = tokens.shape[0]
    top_count = expert_ids.shape[1]
    width = tokens.shape[1]
    normed = rms_scale(tokens.astype(jnp.float32), norm_gain).astype(jnp.bfloat16)
    flat_ids = expert_ids.reshape(-1)
    onehot = (flat_ids[:, None] == jnp.arange(EXPERTS, dtype=jnp.int32)[None, :]).astype(jnp.int32)
    slot_index = jnp.sum(jnp.cumsum(onehot, axis=0) * onehot, axis=1) - 1
    position = flat_ids * CAP + slot_index
    source_row = jnp.arange(tok_count * top_count, dtype=jnp.int32) // top_count
    lookup = jnp.full((EXPERTS * CAP,), tok_count, jnp.int32).at[position].set(source_row)
    padded = jnp.concatenate([normed, jnp.zeros((1, width), jnp.bfloat16)], axis=0)
    outgoing = padded[lookup].reshape(EXPERTS, 1, CAP, width)
    whole_gate, whole_up, whole_down = (
        lax.all_gather(expert_gate, "tp", axis=2, tiled=True),
        lax.all_gather(expert_up, "tp", axis=2, tiled=True),
        lax.all_gather(expert_down, "tp", axis=1, tiled=True),
    )
    arrived = lax.all_to_all(outgoing, "ep", split_axis=0, concat_axis=1, tiled=True)
    local_experts = arrived.shape[0]
    senders = arrived.shape[1]
    slots = arrived.shape[2]
    tok_rows = arrived.reshape(local_experts, senders * slots, width)
    result = expert_rows(tok_rows, whole_gate, whole_up, whole_down).astype(jnp.bfloat16)
    result = result.reshape(local_experts, senders, slots, width)
    returned = lax.all_to_all(result, "ep", split_axis=1, concat_axis=0, tiled=True)
    shared_out = shared_branch(normed, shared_gate, shared_up, shared_down)
    back_rows = returned.reshape(EXPERTS * CAP, width)
    picked = back_rows[position].reshape(tok_count, top_count, width).astype(jnp.float32)
    routed = jnp.einsum("tk,tkd->td", gate_weights, picked)
    combined = routed + shared_out
    return rms_scale(combined, post_gain).astype(jnp.bfloat16)


def solution(mesh):
    return jax.shard_map(
        body,
        mesh=mesh,
        in_specs=(
            P(("grp", "ep", "tp"), None),
            P(),
            P(("grp", "ep", "tp"), None),
            P(("grp", "ep", "tp"), None),
            P("ep", None, "tp"),
            P("ep", None, "tp"),
            P("ep", "tp", None),
            P(),
            P(),
            P(),
            P(),
        ),
        out_specs=P(("grp", "ep", "tp"), None),
        check_vma=False,
    )
```

profile of v0, /device:TPU:37, one launch (start us, length us, event | category | flops | bytes accessed | tf_op | source)
XLA Modules:
  0.0 1045.2 jit_solution(7751365123441853324)
XLA Ops:
  6.6 1.0 copy.18
  7.5 0.1 eq.29
  7.6 0.1 eq.25
  7.8 0.7 broadcast_multiply_fusion
  8.5 9.0 reduce-window.6
  17.5 0.1 slice.12
  17.6 0.1 copy.20
  17.8 0.1 broadcast_add_fusion
  18.0 0.1 copy.17
  18.1 0.1 mul.80
  18.3 4.3 scatter_custom_fusion
  22.6 0.3 fusion.1
  23.0 0.3 fusion.3
  23.3 1.0 copy-done.2
  24.3 6.1 gather_fusion
  30.5 33.2 %all-to-all-start = ((bf16[32,1,40,2048]{3,2,1,0:T(8,128)(2,1)}), bf16[32,1,40,2048]{3,2,1,0:T(8,128)(2,1)}, u32[]{:S(2)}, u32[]{:S(2)}) async-start(bf16[32,1,40,2048]{3,2,1,0:T(8,128)(2,1)} %bitcast.47), calls=%async_computation | async-start | bytes 10485760 | tf_op jit(solution)/shard_map/all_to_all | solution.py:62
  63.7 0.7 all-gather.4.cloned.1.call-update
  64.5 0.7 all-gather.6.cloned.1.call-update
  65.4 0.7 all-gather.8.cloned.1.call-update
  66.1 29.7 %all-gather.4.cloned.1.call-done = bf16[1,2048,512]{2,1,0:T(8,128)(2,1)} async-done(((bf16[1,2048,256]{2,1,0:T(8,128)(2,1)}), bf16[1,2048,512]{2,1,0:T(8,128)(2,1)}) %all-gather.4.cloned.1.call-update) | async-done | bytes 2097168 | tf_op jit(solution)/shard_map/all_gather | solution.py:58
  95.8 417.7 %all-to-all-done = bf16[32,1,40,2048]{3,2,1,0:T(8,128)(2,1)} async-done(((bf16[32,1,40,2048]{3,2,1,0:T(8,128)(2,1)}), bf16[32,1,40,2048]{3,2,1,0:T(8,128)(2,1)}, u32[]{:S(2)}, u32[]{:S(2)}) %all-to-all-start) | async-done | bytes 5242912 | tf_op jit(solution)/shard_map/all_to_all | solution.py:62
  513.5 7.6 fusion.6
  521.1 10.9 %convolution_convert_fusion = bf16[1280,2048]{1,0:T(8,128)(2,1)} fusion(bf16[1,512,2048]{2,1,0:T(8,128)(2,1)} %all-gather.8.cloned.1.call-done, bf16[1280,2048]{1,0:T(8,128)(2,1)} %bitcast.6, f32[1280,512]{1,0:T(8,128)} %fusion.6, bf16[1,2048,512]{2,1,0:T(8,128)(2,1)} %all-gather.6.cloned.1.call-done), kind=kOutput, calls=%fused_computation.3 | convolution fusion | flops 5375262720 | bytes 17301504 | tf_op jit(solution)/shard_map/erf,efd->erd/dot_general | solution.py:22
  532.0 23.2 %all-to-all-start.1 = ((bf16[1,32,40,2048]{3,2,0,1:T(8,128)(2,1)}), bf16[1,32,40,2048]{3,2,0,1:T(8,128)(2,1)}, u32[]{:S(2)}, u32[]{:S(2)}) async-start(bf16[1,32,40,2048]{3,2,0,1:T(8,128)(2,1)} %bitcast.48), calls=%async_computation.1 | async-start | bytes 10485760 | tf_op jit(solution)/shard_map/all_to_all | solution.py:69
  555.2 0.2 copy.24
  555.4 3.1 fusion.28
  558.5 446.8 %all-to-all-done.1 = bf16[1,32,40,2048]{3,2,0,1:T(8,128)(2,1)} async-done(((bf16[1,32,40,2048]{3,2,0,1:T(8,128)(2,1)}), bf16[1,32,40,2048]{3,2,0,1:T(8,128)(2,1)}, u32[]{:S(2)}, u32[]{:S(2)}) %all-to-all-start.1) | async-done | bytes 5242912 | tf_op jit(solution)/shard_map/all_to_all | solution.py:69
  1005.3 12.0 %gather_fusion.1 = bf16[1024,2048]{1,0:T(8,128)(2,1)} fusion(bf16[1280,2048]{1,0:T(8,128)(2,1)} %bitcast.12, s32[1024]{0:T(1024)S(1)} %broadcast_clamp_fusion), kind=kCustom, calls=%fused_computation.1 | custom fusion | bytes 8392704 | tf_op jit(solution)/shard_map/gather | solution.py:72
  1017.4 7.2 reshape.127
  1024.5 5.8 fusion.27
  1030.4 5.4 multiply_reduce_fusion
  1035.8 2.8 multiply_convert_fusion
  (32 shorter events, 0.5 us)
Async XLA Ops:
  6.5 1023.8 %copy-start = (bf16[512,2048]{1,0:T(8,128)(2,1)S(1)}, bf16[512,2048]{1,0:T(8,128)(2,1)}, u32[]{:S(2)}) copy-start(bf16[512,2048]{1,0:T(8,128)(2,1)} %param.20) | copy-start | bytes 6291460
  6.6 16.1 %copy-start.1 = (bf16[256,2048]{1,0:T(8,128)(2,1)S(1)}, bf16[256,2048]{1,0:T(8,128)(2,1)}, u32[]{:S(2)}) copy-start(bf16[256,2048]{1,0:T(8,128)(2,1)} %param.11) | copy-start | bytes 3145732
  6.6 16.4 %copy-start.4 = (f32[2048]{0:T(1024)S(1)}, f32[2048]{0:T(1024)}, u32[]{:S(2)}) copy-start(f32[2048]{0:T(1024)} %param.12) | copy-start | bytes 24580
  23.3 1.0 copy-start.2
  30.5 483.1 %all-to-all-start = ((bf16[32,1,40,2048]{3,2,1,0:T(8,128)(2,1)}), bf16[32,1,40,2048]{3,2,1,0:T(8,128)(2,1)}, u32[]{:S(2)}, u32[]{:S(2)}) async-start(bf16[32,1,40,2048]{3,2,1,0:T(8,128)(2,1)} %bitcast.47), calls=%async_computation | async-start | bytes 10485760 | tf_op jit(solution)/shard_map/all_to_all | solution.py:62
  63.7 32.1 %all-gather.4.cloned.1.call-start = ((), (), s32[]{:S(2)}) async-start(), calls=%async_computation.2 | async-start | bytes 3145728 | tf_op jit(solution)/shard_map/all_gather | solution.py:58
  64.5 456.6 %all-gather.6.cloned.1.call-start = ((), (), s32[]{:S(2)}) async-start(), calls=%async_computation.3 | async-start | bytes 3145728 | tf_op jit(solution)/shard_map/all_gather | solution.py:59
  65.3 455.8 %all-gather.8.cloned.1.call-start = ((), (), s32[]{:S(2)}) async-start(), calls=%async_computation.4 | async-start | bytes 3145728 | tf_op jit(solution)/shard_map/all_gather | solution.py:60
  532.0 23.2 %copy-start.6 = (f32[256,4]{0,1:T(4,128)S(1)}, f32[256,4]{0,1:T(4,128)}, u32[]{:S(2)}) copy-start(f32[256,4]{0,1:T(4,128)} %param.14) | copy-start | bytes 12292
  532.0 23.4 %copy-start.3 = (bf16[256,2048]{1,0:T(8,128)(2,1)S(1)}, bf16[256,2048]{1,0:T(8,128)(2,1)}, u32[]{:S(2)}) copy-start(bf16[256,2048]{1,0:T(8,128)(2,1)} %copy-done.2) | copy-start | bytes 3145732
  532.0 473.3 %all-to-all-start.1 = ((bf16[1,32,40,2048]{3,2,0,1:T(8,128)(2,1)}), bf16[1,32,40,2048]{3,2,0,1:T(8,128)(2,1)}, u32[]{:S(2)}, u32[]{:S(2)}) async-start(bf16[1,32,40,2048]{3,2,0,1:T(8,128)(2,1)} %bitcast.48), calls=%async_computation.1 | async-start | bytes 10485760 | tf_op jit(solution)/shard_map/all_to_all | solution.py:69
  1030.4 5.5 copy-start.5
Sparse Core Ops, SparseCore 0:
  66.3 29.4 all-gather.3
  97.6 28.3 all-gather.5
  127.9 28.8 all-gather.7
where the time goes:
time: 1060 us; the launch traced here: 1050 us
  waiting for transfers between devices  896 us (85%)
  starting transfers between devices  56.6 us (5%)
  matrix products  32.8 us (3%)
  local copies, waits for them, and re-layouts  32.6 us (3%)
  other arithmetic  13.3 us (1%)
  between operations  13.3 us (1%)
    all_to_all x1, waiting for transfers between devices, body(): lax.all_to_all(result, 'ep', split_axis=1, concat_axis=0, tiled=True)  447 us
    all_to_all x1, waiting for transfers between devices, body(): lax.all_to_all(outgoing, 'ep', split_axis=0, concat_axis=1, tiled=True)  418 us
    all_to_all x1, starting transfers between devices, body(): lax.all_to_all(outgoing, 'ep', split_axis=0, concat_axis=1, tiled=True)  33.2 us
    all_gather x1, waiting for transfers between devices, body(): lax.all_gather(expert_gate, 'tp', axis=2, tiled=True)  29.7 us
    all_to_all x1, starting transfers between devices, body(): lax.all_to_all(result, 'ep', split_axis=1, concat_axis=0, tiled=True)  23.2 us
  transfers between devices with their start and end apart: 5, of which 3 were waited for; matrix products, arithmetic and copies ran while one was open for 1% of the time, Pallas kernels for 0%

commit v1 on v0

v1 whole, which is shorter than its diff:
```python
import jax
import jax.numpy as jnp
from jax import lax
from jax.experimental import pallas as pl
from jax.experimental.pallas import tpu as pltpu
from jax.sharding import PartitionSpec as P

EPS = 1e-06
STRIDE = 4
MESH = pl.DeviceIdType.MESH
F32 = jnp.float32
BF16 = jnp.bfloat16


def rms_scale(inputs, gain):
    mean_sq = jnp.mean(inputs * inputs, axis=-1, keepdims=True)
    return inputs * lax.rsqrt(mean_sq + EPS) * gain


def row_length(mesh):
    coords = [getattr(d, "coords", None) for d in mesh.devices.reshape(mesh.devices.shape[0], -1)[:, 0]]
    groups = len(coords)
    if any(c is None for c in coords):
        return 1
    across = len({c[0] for c in coords})
    return across if groups % across == 0 else 1


def silu_mul(g, u):
    return g / (1.0 + jnp.exp(-g)) * u


def dot(a, b):
    return jnp.dot(a, b, preferred_element_type=F32)


def make_kernel(groups, across, ep, blk, width, fh):
    hosts = ep // STRIDE
    half = hosts // 2
    share = width // groups
    hb = blk // 2
    full_steps = (groups - 1) // 2
    steps = groups // 2

    def kernel(
        x_ref, gate_ref, up_ref, down_ref, sg_ref, su_ref, sd_ref,
        own_ref, back_ref, wall_ref,
        xs, acc, wb, sgb, sub, sdb, part,
        disp_s, disp_r, rel_s, rel_r, ch_s, ch_r, xy_s, xy_r, dd_s, dd_r, cb_s, cb_r, ld,
    ):
        grp = lax.axis_index("grp")
        z = lax.axis_index("ep")
        core = lax.axis_index("tp")
        other = 1 - core

        def place(g):
            row, col = g // across, g % across
            return row * across + (col if across == 1 else jnp.where(row % 2 == 0, col, across - 1 - col))

        pos = place(grp)
        nxt = place(lax.rem(pos + 1, groups))
        prv = place(lax.rem(pos + groups - 1, groups))

        def zat(d):
            return lax.rem(z + d + ep, ep)

        own_w = (gate_ref, up_ref, down_ref)
        peers = [{"ep": zat(d)} for d in (1, -1, 2, -2, STRIDE, -STRIDE)]
        peers += [{"tp": other}]
        if groups > 1:
            peers += [{"grp": nxt}, {"grp": prv}]
        barrier = pltpu.get_barrier_semaphore()
        for peer in peers:
            pl.semaphore_signal(barrier, inc=1, device_id=peer, device_id_type=MESH)
        pl.semaphore_wait(barrier, len(peers))

        def remote(src, dst, s, r, to):
            return pltpu.make_async_remote_copy(
                src_ref=src, dst_ref=dst, send_sem=s, recv_sem=r, device_id=to, device_id_type=MESH
            )

        sent = []

        def go(copy):
            copy.start()
            sent.append(copy)

        def dispatch(d, h):
            rows = pl.ds(h * hb, hb)
            return remote(
                x_ref.at[rows], xs.at[1 + d, rows], disp_s.at[d, h], disp_r.at[d, h],
                {"ep": zat(1 - 2 * d)},
            )

        def relay(d):
            rows = pl.ds(d * hb, hb)
            return remote(
                xs.at[1 + d, rows], xs.at[3, rows], rel_s.at[d], rel_r.at[d], {"ep": zat(1 - 2 * d)}
            )

        def slot_of(d, t):
            return t if d == 0 else hosts - t

        def rows_of(region, d, cut):
            if not cut:
                return pl.ds(region * share, share)
            return pl.ds(region * share + d * (share // 2), share // 2)

        def chain(d, m, t):
            rows = rows_of(pos, d, t == half)
            src = own_w[m].at[rows] if t == 1 else wall_ref.at[slot_of(d, t - 1), m, core, rows]
            return remote(
                src, wall_ref.at[slot_of(d, t), m, core, rows], ch_s.at[d, m, t - 1],
                ch_r.at[d, m, t - 1], {"ep": zat(STRIDE * (1 - 2 * d))},
            )

        def exchange(slot, m, j, d, cut, arriving):
            back = j if arriving else j - 1
            region = lax.rem(pos + (groups - back if d == 0 else back), groups)
            rows = rows_of(region, d, cut)
            ref = wall_ref.at[slot, m, core, rows]
            return remote(
                ref, ref, xy_s.at[slot, m, j - 1, d], xy_r.at[slot, m, j - 1, d],
                {"grp": nxt if d == 0 else prv},
            )

        def swap(slot, m):
            dst = wall_ref.at[slot, m, core]
            src = own_w[m] if slot == 0 else dst
            return remote(src, dst, dd_s.at[slot, m], dd_r.at[slot, m], {"tp": other})

        for h in range(2):
            for d in range(2):
                go(dispatch(d, h if d == 0 else 1 - h))
        for m in range(3):
            for d in range(2):
                go(chain(d, m, 1))
        for m in range(3):
            go(swap(0, m))

        loads = [
            pltpu.make_async_copy(a, b, ld.at[i])
            for i, (a, b) in enumerate(((sg_ref, sgb), (su_ref, sub), (sd_ref, sdb)))
        ]
        loads += [pltpu.make_async_copy(own_w[m], wb.at[m, core], ld.at[3 + m]) for m in range(3)]
        for load in loads:
            load.start()
        xs[0] = x_ref[...]
        for b in range(1, 4):
            acc[b] = jnp.zeros((blk, width), F32)
        for load in loads[:3]:
            load.wait()

        def shared():
            x = xs[0, :, :width]
            h = silu_mul(dot(x, sgb[...]), dot(x, sub[...])).astype(BF16)

            @pl.loop(0, width // fh)
            def _(j):
                cols = pl.ds(pl.multiple_of(j * fh, fh), fh)
                acc[0, :, cols] = dot(h, sdb[:, cols])

        shared()

        for d in range(2):
            dispatch(d, d).wait_recv()
            go(relay(d))
        for d in range(2):
            dispatch(d, 1 - d).wait_recv()
        for load in loads[3:]:
            load.wait()

        def block(slot, b, dst=None):
            expert = lax.rem(z + ep - STRIDE * slot, ep)
            x = xs[b, :, :width]
            lane = lax.broadcasted_iota(jnp.int32, (blk, 128), 1)
            pick = (lane < 3 * ep) & (lane % ep == expert)
            w = jnp.sum(jnp.where(pick, xs[b, :, width:].astype(F32), 0.0), axis=1, keepdims=True)
            hidden = [
                (silu_mul(dot(x, wb[0, c]), dot(x, wb[1, c])) * w).astype(BF16) for c in range(2)
            ]
            for j in range(width // fh):
                cols = slice(j * fh, (j + 1) * fh)
                total = acc[b, :, cols] + (
                    dot(hidden[0], wb[2, 0, cols, :]) + dot(hidden[1], wb[2, 1, cols, :])
                )
                if dst is None:
                    acc[b, :, cols] = total
                else:
                    dst[:, cols] = total.astype(dst.dtype)

        def compute(slot):
            @pl.loop(0, 4)
            def _(b):
                block(slot, b)

        def load_slot(slot):
            for m in range(3):
                swap(slot, m).wait_recv()
            copy = pltpu.make_async_copy(wall_ref.at[slot], wb, ld.at[0])
            copy.start()
            copy.wait()

        for m in range(3):
            swap(0, m).wait_recv()
        theirs = [
            pltpu.make_async_copy(wall_ref.at[0, m, other], wb.at[m, other], ld.at[m]) for m in range(3)
        ]
        for load in theirs:
            load.start()
        for load in theirs:
            load.wait()
        for d in range(2):
            relay(d).wait_recv()
        compute(0)

        ready = []
        for t in range(1, half + 1):
            slots = [slot_of(0, t)] if t == half else [slot_of(0, t), slot_of(1, t)]
            for m in range(3):
                for d in range(2):
                    chain(d, m, t).wait_recv()
                    if t < half:
                        go(chain(d, m, t + 1))
                cuts = [False] * full_steps + [True] * (steps - full_steps)
                for j, cut in enumerate(cuts, 1):
                    for slot in slots:
                        for d in range(2):
                            if j > 1:
                                exchange(slot, m, j - 1, d, cuts[j - 2], True).wait_recv()
                        for d in range(2):
                            go(exchange(slot, m, j, d, cut, False))
                    if j == 1 and ready:
                        done = ready.pop(0)
                        load_slot(done)
                        compute(done)
                for slot in slots:
                    for d in range(2):
                        if steps:
                            exchange(slot, m, steps, d, cuts[-1], True).wait_recv()
                    go(swap(slot, m))
            ready += slots
        while len(ready) > 1:
            done = ready.pop(0)
            load_slot(done)
            compute(done)

        last = ready.pop(0)
        load_slot(last)

        def combine(i):
            if i < 2:
                return remote(
                    part.at[i], back_ref.at[i], cb_s.at[i], cb_r.at[i], {"ep": zat(-1 if i == 0 else 1)}
                )
            rows = pl.ds((i - 2) * hb, hb)
            return remote(
                part.at[2, rows], back_ref.at[2, rows], cb_s.at[i], cb_r.at[i],
                {"ep": zat(-2 if i == 2 else 2)},
            )

        block(last, 3, part.at[2])
        block(last, 1, part.at[0])
        go(combine(2))
        go(combine(3))
        block(last, 2, part.at[1])
        go(combine(0))
        block(last, 0, own_ref)
        go(combine(1))
        for i in range(4):
            combine(i).wait_recv()
        for copy in sent:
            copy.wait_send()

    dma = pltpu.SemaphoreType.DMA
    nsteps = max(steps, 1)
    scratch = [
        pltpu.VMEM((4, blk, width + 128), BF16),
        pltpu.VMEM((4, blk, width), F32),
        pltpu.VMEM((3, 2, width, fh), BF16),
        pltpu.VMEM((width, 2 * fh), BF16),
        pltpu.VMEM((width, 2 * fh), BF16),
        pltpu.VMEM((2 * fh, width), BF16),
        pltpu.VMEM((3, blk, width), BF16),
        dma((2, 2)), dma((2, 2)), dma((2,)), dma((2,)),
        dma((2, 3, half)), dma((2, 3, half)),
        dma((hosts, 3, nsteps, 2)), dma((hosts, 3, nsteps, 2)),
        dma((hosts, 3)), dma((hosts, 3)),
        dma((4,)), dma((4,)),
        dma((6,)),
    ]
    anywhere = pl.BlockSpec(memory_space=pl.ANY)
    vmem = pl.BlockSpec(memory_space=pltpu.VMEM)
    return pl.pallas_call(
        kernel,
        out_shape=(
            jax.ShapeDtypeStruct((blk, width), F32),
            jax.ShapeDtypeStruct((3, blk, width), BF16),
            jax.ShapeDtypeStruct((hosts, 3, 2, width, fh), BF16),
        ),
        in_specs=[vmem] + [anywhere] * 6,
        out_specs=(vmem, anywhere, anywhere),
        scratch_shapes=scratch,
        compiler_params=pltpu.CompilerParams(
            collective_id=0, has_side_effects=True, vmem_limit_bytes=60 * 1024 * 1024
        ),
    )


def solution(mesh):
    groups, ep = mesh.shape["grp"], mesh.shape["ep"]
    across = row_length(mesh)

    def body(
        tokens, norm_gain, expert_ids, gate_weights, expert_gate, expert_up, expert_down,
        shared_gate, shared_up, shared_down, post_gain,
    ):
        blk, width = tokens.shape
        fh = expert_gate.shape[2]
        normed = rms_scale(tokens.astype(F32), norm_gain).astype(BF16)
        experts = jnp.arange(ep, dtype=jnp.int32)[None, None, :]
        table = jnp.sum(jnp.where(expert_ids[:, :, None] == experts, gate_weights[:, :, None], 0.0), axis=1)
        high = lax.reduce_precision(table, 8, 7)
        rest = table - high
        middle = lax.reduce_precision(rest, 8, 7)
        low = rest - middle
        pad = jnp.zeros((blk, 128 - 3 * ep), F32)
        extra = jnp.concatenate([high, middle, low, pad], axis=1).astype(BF16)
        rows = jnp.concatenate([normed, extra], axis=1)
        down = expert_down[0].reshape(fh, width // fh, fh).transpose(1, 0, 2).reshape(width, fh)
        own, back, _ = make_kernel(groups, across, ep, blk, width, fh)(
            rows, expert_gate[0], expert_up[0], down, shared_gate, shared_up, shared_down
        )
        combined = own + jnp.sum(back.astype(F32), axis=0)
        return rms_scale(combined, post_gain).astype(BF16)

    rows_spec = P(("grp", "ep", "tp"), None)
    return jax.shard_map(
        body,
        mesh=mesh,
        in_specs=(
            rows_spec, P(), rows_spec, rows_spec,
            P("ep", None, "tp"), P("ep", None, "tp"), P("ep", "tp", None),
            P(), P(), P(), P(),
        ),
        out_specs=rows_spec,
        check_vma=False,
    )
```

time: 1060 us -> 432 us (0.41); the launches traced: 1050 us -> 429 us
  waiting for transfers between devices: 896 us -> 0 us
  Pallas kernels: 0 us -> 417 us
  starting transfers between devices: 56.6 us -> 0 us
  matrix products: 32.8 us -> 0 us
  local copies, waits for them, and re-layouts: 32.6 us -> 4.04 us
  between operations: 13.3 us -> 0.1 us
    all_to_all x2 -> x0, waiting for transfers between devices: 865 us -> none  [the longest x1 447 us: body(): lax.all_to_all(result, 'ep', split_axis=1, concat_axis=0, tiled=True)]
    pallas_call x0 -> x1, Pallas kernels: none -> 417 us  [body(): make_kernel(groups, across, ep, blk, width, fh)]
    all_to_all x2 -> x0, starting transfers between devices: 56.4 us -> none  [the longest x1 33.2 us: body(): lax.all_to_all(outgoing, 'ep', split_axis=0, concat_axis=1, tiled=True)]
    dot_general x5 -> x0, matrix products: 32.8 us -> none  [the longest x1 10.9 us: expert_rows(): jnp.einsum('erf,efd->erd', hidden, w_down, preferred_element_type=jnp.flo...]
    all_gather x3 -> x0, waiting for transfers between devices: 29.7 us -> none  [the longest x1 29.7 us: body(): lax.all_gather(expert_gate, 'tp', axis=2, tiled=True)]
    gather x2 -> x0, local copies, waits for them, and re-layouts: 18.1 us -> none  [the longest x1 12 us: body(): back_rows[position].reshape(tok_count, top_count, width).astype(jnp.float32)]
  transfers between devices with their start and end apart: 5 -> 0, of which waited for: 3 -> 0; matrix products, arithmetic and copies ran while one was open for 1% -> 0% of each run, Pallas kernels for 0% -> 0%
where the time goes in v1:
time: 432 us; the launch traced here: 429 us
  Pallas kernels  417 us (97%)
  other arithmetic  7.85 us (2%)
    pallas_call x1, Pallas kernels, body(): make_kernel(groups, across, ep, blk, width, fh)  417 us

profile of v1, /device:TPU:37, one launch (start us, length us, event | category | flops | bytes accessed | tf_op | source)
XLA Modules:
  0.0 429.2 jit_solution(7607577929227536640)
XLA Ops:
  0.0 0.0 copy-start
  0.0 1.6 fusion
  1.6 0.7 select_reduce_fusion
  2.4 0.1 copy.19
  2.5 0.1 copy.18
  2.6 0.0 copy-done
  2.6 0.0 copy-start.2
  2.6 1.1 fusion.2
  3.7 2.0 concatenate.6.x_ref
  5.7 0.0 copy-done.2
  5.7 0.3 copy.22
  6.0 1.2 copy.21
  7.2 417.2 %shard_map.109 = (f32[256,2048]{1,0:T(8,128)}, bf16[3,256,2048]{2,1,0:T(8,128)(2,1)}, bf16[8,3,2,2048,256]{4,3,2,1,0:T(8,128)(2,1)}) custom-call(bf16[256,2176]{1,0:T(8,128)(2,1)} %concatenate.6.x_ref, bf16[2048,256]{1,0:T(8,128)(2,1)} %bitcast.10, bf16[2048,256]{1,0:T(8,128)(2,1)} %bitcast.11, bf16[2048,256]{1,0:T(8,128)(2,1)} %bitcast.8, ...), custom_call_target="tpu_custom_call" | custom-call | tf_op jit(solution)/shard_map/pallas_call | solution.py:331
  424.4 0.0 copy-start.1
  424.4 2.8 convert_reduce_fusion
  427.3 0.0 copy-done.1
  427.3 0.0 copy-start.3
  427.3 0.3 multiply_reduce_fusion
  427.6 0.4 copy-done.3
  428.0 1.2 multiply_convert_fusion
  (5 shorter events, 0.1 us)
Async XLA Ops:
  0.0 2.6 copy-start
  2.6 3.1 copy-start.2
  424.4 2.9 copy-start.1
  427.3 0.7 copy-start.3

commit v2 on v1

v2 whole, which is shorter than its diff:
```python
import jax
import jax.numpy as jnp
from jax import lax
from jax.experimental import pallas as pl
from jax.experimental.pallas import tpu as pltpu
from jax.sharding import PartitionSpec as P

EPS = 1e-06
STRIDE = 4
MESH = pl.DeviceIdType.MESH
F32 = jnp.float32
BF16 = jnp.bfloat16


def rms_scale(inputs, gain):
    mean_sq = jnp.mean(inputs * inputs, axis=-1, keepdims=True)
    return inputs * lax.rsqrt(mean_sq + EPS) * gain


def row_length(mesh):
    coords = [getattr(d, "coords", None) for d in mesh.devices.reshape(mesh.devices.shape[0], -1)[:, 0]]
    groups = len(coords)
    if any(c is None for c in coords):
        return 1
    across = len({c[0] for c in coords})
    return across if groups % across == 0 else 1


def silu_mul(g, u):
    return g / (1.0 + jnp.exp(-g)) * u


def dot(a, b):
    return jnp.dot(a, b, preferred_element_type=F32)


def make_kernel(groups, across, ep, blk, width, fh, top):
    hosts = ep // STRIDE
    half = hosts // 2
    share = width // groups
    hb = blk // 2
    chunk = 32
    full_steps = (groups - 1) // 2
    steps = groups // 2
    cuts = [False] * full_steps + [True] * (steps - full_steps)

    def kernel(
        tok_ref, gain_ref, ids_ref, gw_ref, post_ref,
        gate_ref, up_ref, down_ref, sg_ref, su_ref, sd_ref,
        out_ref, wall_ref,
        xs, acc, wb, sgb, sub, sdb, part, inbox, back, hid,
        disp_s, disp_r, rel_s, rel_r, ch_s, ch_r, xy_s, xy_r, dd_s, dd_r, cb_s, cb_r, ld, lw, pace,
    ):
        grp = lax.axis_index("grp")
        z = lax.axis_index("ep")
        core = lax.axis_index("tp")
        other = 1 - core

        def place(g):
            row, col = g // across, g % across
            return row * across + (col if across == 1 else jnp.where(row % 2 == 0, col, across - 1 - col))

        pos = place(grp)
        nxt = place(lax.rem(pos + 1, groups))
        prv = place(lax.rem(pos + groups - 1, groups))

        def zat(d):
            return lax.rem(z + d + ep, ep)

        own_w = (gate_ref, up_ref, wb.at[0, 2, core])
        peers = [{"ep": zat(d)} for d in (1, -1, STRIDE, -STRIDE)]
        peers += [{"tp": other}]
        if groups > 1:
            peers += [{"grp": nxt}, {"grp": prv}]
        barrier = pltpu.get_barrier_semaphore()
        for peer in peers:
            pl.semaphore_signal(barrier, inc=1, device_id=peer, device_id_type=MESH)

        loads = [
            pltpu.make_async_copy(gate_ref, wb.at[0, 0, core], ld.at[0]),
            pltpu.make_async_copy(up_ref, wb.at[0, 1, core], ld.at[1]),
        ]
        for j in range(width // fh):
            cols = slice(j * fh, (j + 1) * fh)
            loads.append(pltpu.make_async_copy(down_ref.at[:, cols], wb.at[0, 2, core, cols], ld.at[2 + j]))
        for i, (a, b) in enumerate(((sg_ref, sgb), (su_ref, sub), (sd_ref, sdb))):
            loads.append(pltpu.make_async_copy(a, b, ld.at[2 + width // fh + i]))
        for load in loads:
            load.start()
        with jax.named_scope("entry"):
            pl.semaphore_wait(barrier, len(peers))

        def remote(src, dst, s, r, to):
            return pltpu.make_async_remote_copy(
                src_ref=src, dst_ref=dst, send_sem=s, recv_sem=r, device_id=to, device_id_type=MESH
            )

        sent = []

        def go(copy):
            copy.start()
            sent.append(copy)

        def dispatch(d, h):
            rows = pl.ds(h * hb, hb)
            return remote(
                xs.at[0, rows], xs.at[1 + d, rows], disp_s.at[d, h], disp_r.at[d, h],
                {"ep": zat(1 - 2 * d)},
            )

        def relay(d):
            rows = pl.ds(d * hb, hb)
            return remote(
                xs.at[1 + d, rows], xs.at[3, rows], rel_s.at[d], rel_r.at[d], {"ep": zat(1 - 2 * d)}
            )

        def slot_of(d, t):
            return t if d == 0 else hosts - t

        def rows_of(region, d, cut):
            if not cut:
                return pl.ds(region * share, share)
            return pl.ds(region * share + d * (share // 2), share // 2)

        def chain(d, m, t):
            rows = rows_of(pos, d, t == half)
            src = own_w[m].at[rows] if t == 1 else wall_ref.at[slot_of(d, t - 1), m, core, rows]
            return remote(
                src, wall_ref.at[slot_of(d, t), m, core, rows], ch_s.at[d, m, t - 1],
                ch_r.at[d, m, t - 1], {"ep": zat(STRIDE * (1 - 2 * d))},
            )

        def exchange(slot, m, j, d, arriving):
            back_by = j if arriving else j - 1
            region = lax.rem(pos + (groups - back_by if d == 0 else back_by), groups)
            ref = wall_ref.at[slot, m, core, rows_of(region, d, cuts[j - 1])]
            return remote(
                ref, ref, xy_s.at[slot, m, j - 1, d], xy_r.at[slot, m, j - 1, d],
                {"grp": nxt if d == 0 else prv},
            )

        def exchange_wait(slots, m, j):
            for slot in slots:
                for d in range(2):
                    exchange(slot, m, j, d, True).wait_recv()

        def exchange_start(slots, m, j):
            for slot in slots:
                for d in range(2):
                    go(exchange(slot, m, j, d, False))

        def swap(slot, m):
            dst = wall_ref.at[slot, m, core]
            src = own_w[m] if slot == 0 else dst
            return remote(src, dst, dd_s.at[slot, m], dd_r.at[slot, m], {"tp": other})

        def finish(slots, m):
            if steps:
                exchange_wait(slots, m, steps)
            for slot in slots:
                go(swap(slot, m))

        for d in range(2):
            go(chain(d, 0, 1))

        lane = lax.broadcasted_iota(jnp.int32, (chunk, 128), 1)

        @pl.loop(0, blk // chunk)
        def _(i):
            rows = pl.ds(pl.multiple_of(i * chunk, chunk), chunk)
            x = tok_ref[rows, :].astype(F32)
            xs[0, rows, :width] = rms_scale(x, gain_ref[...]).astype(BF16)
            table = jnp.zeros((chunk, 128), F32)
            for k in range(top):
                table += jnp.where(ids_ref[rows, k : k + 1] == lane % ep, gw_ref[rows, k : k + 1], 0.0)
            high = table.astype(BF16).astype(F32)
            middle = (table - high).astype(BF16).astype(F32)
            low = table - high - middle
            extra = jnp.where(lane < ep, high, jnp.where(lane < 2 * ep, middle, low))
            xs[0, rows, width:] = jnp.where(lane < 3 * ep, extra, 0.0).astype(BF16)

        for load in loads:
            load.wait()

        x = xs[0, :, :width]
        shared_hidden = silu_mul(dot(x, sgb[...]), dot(x, sub[...])).astype(BF16)

        for h in range(2):
            for d in range(2):
                go(dispatch(d, h if d == 0 else 1 - h))
        for d in range(2):
            go(chain(d, 1, 1))
        for m in range(3):
            go(swap(0, m))
        from_wb = sent[-1:]

        for j in range(width // (2 * fh)):
            cols = slice(j * 2 * fh, (j + 1) * 2 * fh)
            acc[0, :, cols] = dot(shared_hidden, sdb[:, cols])
        for b in range(1, 4):
            acc[b] = jnp.zeros((blk, width), F32)

        order = [0] + [slot_of(d, t) for t in range(1, half) for d in range(2)] + [half]
        turn = {slot: i % 2 for i, slot in enumerate(order)}

        def hidden(slot, b):
            expert = lax.rem(z + ep - STRIDE * slot, ep)
            x = xs[b, :, :width]
            w1 = wb.at[turn[slot]]
            lanes = lax.broadcasted_iota(jnp.int32, (blk, 128), 1)
            pick = (lanes < 3 * ep) & (lanes % ep == expert)
            w = jnp.sum(jnp.where(pick, xs[b, :, width:].astype(F32), 0.0), axis=1, keepdims=True)
            return [(silu_mul(dot(x, w1[0, c]), dot(x, w1[1, c])) * w).astype(BF16) for c in range(2)]

        def down(slot, b, hs, cols):
            w2 = wb.at[turn[slot], 2]
            return acc[b, :, cols] + (dot(hs[0], w2[0, cols, :]) + dot(hs[1], w2[1, cols, :]))

        groups_of_cols = [slice(j * fh, (j + 1) * fh) for j in range(width // fh)]

        def compute(slot):
            @pl.loop(0, 4)
            def _(b):
                hs = hidden(slot, b)
                for cols in groups_of_cols:
                    acc[b, :, cols] = down(slot, b, hs, cols)

        def compute_hidden(slot):
            @pl.loop(0, 4)
            def _(b):
                for c, h in enumerate(hidden(slot, b)):
                    hid[turn[slot], b, c] = h

        def compute_down(slot):
            @pl.loop(0, 4)
            def _(b):
                hs = [hid[turn[slot], b, c] for c in range(2)]
                for cols in groups_of_cols:
                    acc[b, :, cols] = down(slot, b, hs, cols)

        def loading(slot, ms):
            return [
                pltpu.make_async_copy(wall_ref.at[slot, m], wb.at[turn[slot], m], lw.at[turn[slot], m])
                for m in ms
            ]

        def load_start(slot, ms):
            for m in ms:
                swap(slot, m).wait_recv()
            for copy in loading(slot, ms):
                copy.start()

        def load_wait(slot, ms):
            for copy in loading(slot, ms):
                copy.wait()

        def first_slot():
            for m in range(3):
                swap(0, m).wait_recv()
            theirs = [
                pltpu.make_async_copy(wall_ref.at[0, m, other], wb.at[0, m, other], ld.at[m])
                for m in range(3)
            ]
            for load in theirs:
                load.start()
            for d in range(2):
                dispatch(d, 1 - d).wait_recv()
            for d in range(2):
                relay(d).wait_recv()
            for load in theirs:
                load.wait()
            compute(0)

        def advance(slots, m):
            for j in range(2, steps + 1):
                exchange_wait(slots, m, j - 1)
                exchange_start(slots, m, j)

        for d in range(2):
            dispatch(d, d).wait_recv()
            go(relay(d))
        for d in range(2):
            go(chain(d, 2, 1))
        from_wb += sent[-2:]

        last = order[-1]

        def pair_hidden(slots):
            for slot in slots:
                load_start(slot, (0, 1))
            for slot in slots:
                load_wait(slot, (0, 1))
                compute_hidden(slot)

        def pair_down(slots):
            for copy in from_wb:
                copy.wait_send()
                sent[:] = [c for c in sent if c is not copy]
            from_wb.clear()
            for slot in slots:
                load_start(slot, (2,))
            for slot in slots:
                load_wait(slot, (2,))
                compute_down(slot)

        def pace_signal():
            for d in range(2):
                pl.semaphore_signal(pace.at[d], inc=1, device_id={"ep": zat(1 - 2 * d)}, device_id_type=MESH)

        def pace_wait():
            for d in range(2):
                pl.semaphore_wait(pace.at[d], 1)

        previous = None
        for t in range(1, half + 1):
            slots = [slot_of(0, t)] if t == half else [slot_of(0, t), slot_of(1, t)]
            pair = [slot_of(0, t - 1), slot_of(1, t - 1)]
            for m in range(3):
                if previous is not None:
                    with jax.named_scope(f"advance{t}{m}"):
                        advance(*previous)
                with jax.named_scope(f"chain{t}{m}"):
                    for d in range(2):
                        chain(d, m, t).wait_recv()
                with jax.named_scope(f"pace{t}{m}"):
                    pace_signal()
                    if previous is not None:
                        pace_wait()
                if t < half:
                    for d in range(2):
                        go(chain(d, m, t + 1))
                if steps:
                    exchange_start(slots, m, 1)
                with jax.named_scope(f"compute{t}{m}"):
                    if t == 1 and m == 1:
                        first_slot()
                    elif t > 1 and m == 0:
                        pair_hidden(pair)
                    elif t > 1 and m == 1:
                        pair_down(pair)
                if previous is not None:
                    with jax.named_scope(f"finish{t}{m}"):
                        finish(*previous)
                previous = (slots, m)

        pace_wait()
        with jax.named_scope("drain"):
            load_start(last, (0,))
            advance(*previous)
        with jax.named_scope("last_hidden"):
            load_start(last, (1,))
            load_wait(last, (0, 1))
            compute_hidden(last)
        with jax.named_scope("last_finish"):
            finish(*previous)
        with jax.named_scope("last_load"):
            load_start(last, (2,))
            load_wait(last, (2,))

        def combine(i):
            d = i % 2
            early = i < 4
            rows = pl.ds((d if i < 2 or not early else 1 - d) * hb, hb)
            src, dst = (part.at[2, rows], inbox.at[rows]) if i < 2 else (part.at[d, rows], back.at[d, rows])
            return remote(src, dst, cb_s.at[i], cb_r.at[i], {"ep": zat(2 * d - 1)})

        def last_down(b):
            hs = [hid[turn[last], b, c] for c in range(2)]
            for cols in groups_of_cols:
                total = down(last, b, hs, cols)
                if b == 3:
                    part[2, :, cols] = total.astype(BF16)
                elif b == 1:
                    part[0, hb:, cols] = total[hb:].astype(BF16)
                    acc[1, :hb, cols] = total[:hb]
                elif b == 2:
                    part[1, :hb, cols] = total[:hb].astype(BF16)
                    acc[2, hb:, cols] = total[hb:]
                else:
                    acc[0, :, cols] = total

        with jax.named_scope("down31"):
            last_down(3)
            last_down(1)
        with jax.named_scope("send01"):
            go(combine(0))
            go(combine(1))
        with jax.named_scope("down2"):
            last_down(2)
        go(combine(2))
        with jax.named_scope("down0"):
            last_down(0)
        go(combine(3))
        with jax.named_scope("comb0"):
            combine(0).wait_recv()
        with jax.named_scope("add"):
          part[0, :hb, :] = (acc[1, :hb, :] + inbox[:hb, :].astype(F32)).astype(BF16)
        combine(1).wait_recv()
        part[1, hb:, :] = (acc[2, hb:, :] + inbox[hb:, :].astype(F32)).astype(BF16)
        go(combine(4))
        go(combine(5))
        with jax.named_scope("comb"):
            for i in range(2, 6):
                combine(i).wait_recv()

        @pl.loop(0, blk // chunk)
        def _(i):
            rows = pl.ds(pl.multiple_of(i * chunk, chunk), chunk)
            combined = acc[0, rows, :] + back[0, rows, :].astype(F32) + back[1, rows, :].astype(F32)
            out_ref[rows, :] = rms_scale(combined, post_ref[...]).astype(BF16)

        for copy in sent:
            copy.wait_send()

    dma = pltpu.SemaphoreType.DMA
    nsteps = max(steps, 1)
    scratch = [
        pltpu.VMEM((4, blk, width + 128), BF16),
        pltpu.VMEM((4, blk, width), F32),
        pltpu.VMEM((2, 3, 2, width, fh), BF16),
        pltpu.VMEM((width, 2 * fh), BF16),
        pltpu.VMEM((width, 2 * fh), BF16),
        pltpu.VMEM((2 * fh, width), BF16),
        pltpu.VMEM((3, blk, width), BF16),
        pltpu.VMEM((blk, width), BF16),
        pltpu.VMEM((2, blk, width), BF16),
        pltpu.VMEM((2, 4, 2, blk, fh), BF16),
        dma((2, 2)), dma((2, 2)), dma((2,)), dma((2,)),
        dma((2, 3, half)), dma((2, 3, half)),
        dma((hosts, 3, nsteps, 2)), dma((hosts, 3, nsteps, 2)),
        dma((hosts, 3)), dma((hosts, 3)),
        dma((6,)), dma((6,)),
        dma((5 + width // fh,)), dma((2, 3)), pltpu.SemaphoreType.REGULAR((2,)),
    ]
    anywhere = pl.BlockSpec(memory_space=pl.ANY)
    vmem = pl.BlockSpec(memory_space=pltpu.VMEM)
    return pl.pallas_call(
        kernel,
        out_shape=(
            jax.ShapeDtypeStruct((blk, width), BF16),
            jax.ShapeDtypeStruct((hosts, 3, 2, width, fh), BF16),
        ),
        in_specs=[vmem] * 5 + [anywhere] * 6,
        out_specs=(vmem, anywhere),
        scratch_shapes=scratch,
        compiler_params=pltpu.CompilerParams(
            collective_id=0, has_side_effects=True, vmem_limit_bytes=60 * 1024 * 1024
        ),
    )


def solution(mesh):
    groups, ep = mesh.shape["grp"], mesh.shape["ep"]
    across = row_length(mesh)

    def body(
        tokens, norm_gain, expert_ids, gate_weights, expert_gate, expert_up, expert_down,
        shared_gate, shared_up, shared_down, post_gain,
    ):
        blk, width = tokens.shape
        fh = expert_gate.shape[2]
        mixed, _ = make_kernel(groups, across, ep, blk, width, fh, expert_ids.shape[1])(
            tokens, norm_gain[None], expert_ids, gate_weights, post_gain[None],
            expert_gate[0], expert_up[0], expert_down[0], shared_gate, shared_up, shared_down,
        )
        return mixed

    rows_spec = P(("grp", "ep", "tp"), None)
    return jax.shard_map(
        body,
        mesh=mesh,
        in_specs=(
            rows_spec, P(), rows_spec, rows_spec,
            P("ep", None, "tp"), P("ep", None, "tp"), P("ep", "tp", None),
            P(), P(), P(), P(),
        ),
        out_specs=rows_spec,
        check_vma=False,
    )
```

time: 432 us -> 395 us (0.914)
  Pallas kernels: 417 us -> 389 us
  other arithmetic: 7.85 us -> 0 us
    pallas_call x1, Pallas kernels: 417 us -> 389 us  [body(): make_kernel(groups, across, ep, blk, width, fh, expert_ids.shape[1])]
    reduce_sum x4 -> x0, other arithmetic: 5.49 us -> none  [the longest x1 2.85 us: body(): combined = own + jnp.sum(back.astype(F32), axis=0)]
    unnamed x9 -> x3, local copies, waits for them, and re-layouts: 0.68 us -> 5.26 us
where the time goes in v2:
time: 395 us; the launch traced here: 394 us
  Pallas kernels  389 us (98%)
  local copies, waits for them, and re-layouts  5.26 us (1%)
    pallas_call x1, Pallas kernels, body(): make_kernel(groups, across, ep, blk, width, fh, expert_ids.shape[1])  389 us

profile of v2, /device:TPU:37, one launch (start us, length us, event | category | flops | bytes accessed | tf_op | source)
XLA Modules:
  0.0 394.5 jit_solution(10252252513036115144)
XLA Ops:
  0.0 1.5 copy.12.ids_ref
  1.5 1.5 copy.13.gw_ref
  3.0 389.2 %shard_map.109 = (bf16[256,2048]{1,0:T(8,128)(2,1)}, bf16[8,3,2,2048,256]{4,3,2,1,0:T(8,128)(2,1)}) custom-call(bf16[256,2048]{1,0:T(8,128)(2,1)} %tok_ref.1, f32[1,2048]{1,0:T(1,128)} %bitcast.8, s32[256,4]{1,0:T(8,128)} %copy.12.ids_ref, f32[256,4]{1,0:T(8,128)} %copy.13.gw_ref, f32[1,2048]{1,0:T(1,128)} %bitcast.9, bf16[2048,256]{1,0:T(8,128)(2,1)} %bitcast.5, ...), custom_call_target="tpu_custom_call" | custom-call | tf_op jit(solution)/shard_map/pallas_call | solution.py:462
  392.1 2.3 copy.15

commit v3 on v2

--- a/solution.py
+++ b/solution.py
@@ -326,9 +326,10 @@
                     pace_signal()
                     if previous is not None:
                         pace_wait()
-                if t < half:
-                    for d in range(2):
-                        go(chain(d, m, t + 1))
+                if t < half and (t, m) != (1, 0):
+                    for late in (0, 1) if (t, m) == (1, 1) else (m,):
+                        for d in range(2):
+                            go(chain(d, late, t + 1))
                 if steps:
                     exchange_start(slots, m, 1)
                 with jax.named_scope(f"compute{t}{m}"):
@@ -394,7 +395,7 @@
         with jax.named_scope("comb0"):
             combine(0).wait_recv()
         with jax.named_scope("add"):
-          part[0, :hb, :] = (acc[1, :hb, :] + inbox[:hb, :].astype(F32)).astype(BF16)
+            part[0, :hb, :] = (acc[1, :hb, :] + inbox[:hb, :].astype(F32)).astype(BF16)
         combine(1).wait_recv()
         part[1, hb:, :] = (acc[2, hb:, :] + inbox[hb:, :].astype(F32)).astype(BF16)
         go(combine(4))

time: 395 us -> 395 us (level)
  no operation moved by 1% of the time
where the time goes in v3:
time: 395 us; the launch traced here: 394 us
  Pallas kernels  389 us (98%)
  local copies, waits for them, and re-layouts  5.26 us (1%)
    pallas_call x1, Pallas kernels, body(): make_kernel(groups, across, ep, blk, width, fh, expert_ids.shape[1])  389 us

profile of v3, /device:TPU:37, one launch (start us, length us, event | category | flops | bytes accessed | tf_op | source)
XLA Modules:
  0.0 394.5 jit_solution(2990094480847401511)
XLA Ops:
  0.0 1.5 copy.12.ids_ref
  1.5 1.5 copy.13.gw_ref
  3.0 389.2 %shard_map.109 = (bf16[256,2048]{1,0:T(8,128)(2,1)}, bf16[8,3,2,2048,256]{4,3,2,1,0:T(8,128)(2,1)}) custom-call(bf16[256,2048]{1,0:T(8,128)(2,1)} %tok_ref.1, f32[1,2048]{1,0:T(1,128)} %bitcast.8, s32[256,4]{1,0:T(8,128)} %copy.12.ids_ref, f32[256,4]{1,0:T(8,128)} %copy.13.gw_ref, f32[1,2048]{1,0:T(1,128)} %bitcast.9, bf16[2048,256]{1,0:T(8,128)(2,1)} %bitcast.5, ...), custom_call_target="tpu_custom_call" | custom-call | tf_op jit(solution)/shard_map/pallas_call | solution.py:463
  392.1 2.3 copy.15
